TPU v7x, 512 devices: a 8x2x16 block of a 8x8x16 slice. The times are simulated.
512 devices in a mesh: grp: 2 (over y), fs: 32 (over z, core), tp: 8 (over x).
Axes of the slice: x: 8, y: 2, z: 16, core: 2. Of those that a mesh axis runs over, the one named last changes fastest.
The devices are a block of a 8x8x16 slice.
Arguments:
- tokens: bfloat16 [24576, 2048], P(('grp', 'fs'), 'tp'), parts along dimension 0, may hold values from -6 to 6
- norm_gain: float32 [2048], P('fs'), may hold values from 0.1 to 1.9
- gate_weight: float32 [32, 2048, 1024], P(None, 'fs', 'tp'), may hold values from -0.125 to 0.125
- up_weight: float32 [32, 2048, 1024], P(None, 'fs', 'tp'), may hold values from -0.125 to 0.125
- down_weight: float32 [32, 1024, 2048], P(None, 'fs', 'tp'), may hold values from -0.1875 to 0.1875
- routes: int32 [24576, 2], P(('grp', 'fs')), parts along dimension 0, may hold values from 0 to 31, as said below
- route_weights: float32 [24576, 2], P(('grp', 'fs')), parts along dimension 0, may hold values from 0.2 to 1
Outputs:
- gate_serve: bfloat16 [64, 2048, 1024], P(('grp', 'fs'), None, 'tp'), parts along dimension 0
- up_serve: bfloat16 [64, 2048, 1024], P(('grp', 'fs'), None, 'tp'), parts along dimension 0
- down_serve: bfloat16 [64, 1024, 2048], P(('grp', 'fs'), None, 'tp'), parts along dimension 0
- mixture: bfloat16 [24576, 2048], P(('grp', 'fs'), 'tp'), parts along dimension 0
There are 2 independent parts, one for each index of `grp`. A program takes and returns all parts, laid end to end along the dimension named above; an argument that names none is the same for every part. Nothing has to cross between parts.
Inputs may be any that keep to these rules, and one draw needn't show every extreme that they name: `routes`: each row names two different experts of one group (expert e lies in group e // 8). In each aligned block of 384 rows no expert is named more than 36 times, and every expert of one group is named exactly 36 times.
All inputs are finite; a program needn't handle non-finite values.
Results may differ from a plain program's by a relative error of at most 0.0087.
Values may be sent and summed in bfloat16 or wider, within the bound.
No kernel may reach another device: no remote copies, remote signals or barrier semaphores. Data moves between devices by JAX's collectives and lax.ppermute only.
A program may use at most 64 MiB of HBM per device.

v0:
```python
import jax
import jax.numpy as jnp
from jax import lax
from jax.sharding import Mesh
from jax.sharding import PartitionSpec as P

CAP = 36
FS = ("fs_0", "fs_1")
GRP_FS = ("grp", "fs_0", "fs_1")
epsilon = 1e-06


def in_blocks(x, dim, length):
    before, after = (x.shape[:dim], x.shape[dim + 1 :])
    return jnp.moveaxis(x.reshape(*before, length, -1, *after), dim, 0)


def laid_out(blocks, dim):
    blocks = jnp.moveaxis(blocks, 0, dim)
    shape = blocks.shape
    return blocks.reshape(*shape[:dim], shape[dim] * shape[dim + 1], *shape[dim + 2 :])


def exchange_in_order(blocks, axes, order):
    shape = [lax.axis_size(a) for a in axes]
    blocks = blocks.reshape(*shape, *blocks.shape[1:])
    for k in order:
        blocks = lax.all_to_all(blocks, axes[k], split_axis=k, concat_axis=k, tiled=True)
    return blocks.reshape(-1, *blocks.shape[len(axes) :])


def exchange_by_chip(x, groups, order, split_dim, concat_dim):
    length = lax.axis_size(groups[0]) * lax.axis_size(groups[1])
    blocks = in_blocks(x, split_dim, length)
    return laid_out(exchange_in_order(blocks, groups, order), concat_dim)


def normalize(rows):
    values = rows.astype(jnp.float32)
    scale = lax.rsqrt(jnp.mean(values * values, axis=-1, keepdims=True) + epsilon)
    return (values * scale).astype(jnp.bfloat16)


def shards(tokens, norm_gain, gate_weight, up_weight, down_weight, routes, route_weights):
    experts = gate_weight.shape[0]
    n_shards = lax.axis_size(FS)
    local_experts = experts // n_shards
    tok_rows = tokens.shape[0]
    gate_low = (norm_gain[None, :, None] * gate_weight).astype(jnp.bfloat16)
    up_low = (norm_gain[None, :, None] * up_weight).astype(jnp.bfloat16)
    down_low = down_weight.astype(jnp.bfloat16)
    gate_serve, up_serve = (
        lax.all_to_all(gate_low, FS, split_axis=0, concat_axis=1, tiled=True),
        lax.all_to_all(up_low, FS, split_axis=0, concat_axis=1, tiled=True),
    )
    flat_routes = routes.reshape(-1)
    expert_ids = lax.iota(jnp.int32, experts)
    onehot = (flat_routes[:, None] == expert_ids[None, :]).astype(jnp.int32)
    position = jnp.sum((jnp.cumsum(onehot, axis=0) - 1) * onehot, axis=1)
    slot_index = (flat_routes * CAP + position).reshape(tok_rows, 2)
    slot_ids = lax.iota(jnp.int32, experts * CAP)
    select = jnp.any(slot_ids[:, None, None] == slot_index[None, :, :], axis=2).astype(jnp.bfloat16)
    outbound = jnp.dot(select, tokens, preferred_element_type=jnp.float32).astype(jnp.bfloat16)
    outbound = outbound.reshape(n_shards, local_experts, CAP, outbound.shape[1])
    arrived = lax.all_to_all(outbound, FS, split_axis=0, concat_axis=2, tiled=True)[0]
    expert_rows = normalize(lax.all_gather(arrived, "tp", axis=2, tiled=True))
    gate_part = jnp.einsum(
        "erd,edh->erh", expert_rows, gate_serve, preferred_element_type=jnp.float32
    )
    up_part = jnp.einsum("erd,edh->erh", expert_rows, up_serve, preferred_element_type=jnp.float32)
    hidden = (jax.nn.silu(gate_part) * up_part).astype(jnp.bfloat16)
    down_serve = lax.all_to_all(down_low, FS, split_axis=0, concat_axis=1, tiled=True)
    expert_out = jnp.einsum(
        "erk,ekd->erd",
        lax.all_gather(hidden, "tp", axis=2, tiled=True),
        down_serve,
        preferred_element_type=jnp.float32,
    ).astype(jnp.bfloat16)
    expert_out = expert_out.reshape(1, local_experts, hidden.shape[1], expert_out.shape[2])
    returned_rows = exchange_by_chip(expert_out, ("fs_0", "fs_1"), (1, 0), 2, 0)
    returned_rows = returned_rows.reshape(experts * CAP, returned_rows.shape[3])
    picked = returned_rows[slot_index]
    mixture = jnp.sum(route_weights[:, :, None] * picked.astype(jnp.float32), axis=1).astype(
        jnp.bfloat16
    )
    return (gate_serve, up_serve, down_serve, mixture)


def solution(mesh):
    split = Mesh(
        mesh.devices.reshape(mesh.shape["grp"], 16, 2, mesh.shape["tp"]),
        ("grp", "fs_0", "fs_1", "tp"),
    )
    placed = (
        P(GRP_FS, "tp"),
        P(FS),
        P(None, FS, "tp"),
        P(None, FS, "tp"),
        P(None, FS, "tp"),
        P(GRP_FS, None),
        P(GRP_FS, None),
    )
    return jax.shard_map(
        shards,
        mesh=split,
        in_specs=placed,
        out_specs=(
            P(GRP_FS, None, "tp"),
            P(GRP_FS, None, "tp"),
            P(GRP_FS, None, "tp"),
            P(GRP_FS, "tp"),
        ),
        check_vma=False,
    )
```

profile of v0, /device:TPU:66, one launch (start us, length us, event | category | flops | bytes accessed | tf_op | source)
XLA Modules:
  0.0 293.5 jit_solution(14518242084303444602)
XLA Ops:
  7.2 0.0 copy-start
  7.2 0.0 copy-start.3
  7.2 0.0 copy-start.5
  7.2 0.1 all-gather.4.cloned.1.call-start
  7.3 0.9 copy.41
  8.2 0.1 eq.43
  8.3 0.1 eq.39
  8.5 1.7 reduce-window.6
  10.3 0.3 slice_reduce_fusion
  10.5 0.1 fusion.9
  10.7 0.2 reduce_sum.30
  10.8 0.1 copy.44
  10.9 0.7 compare_select_fusion
  11.6 0.8 fusion.3
  12.4 0.0 copy-done
  12.4 0.5 convolution_convert_fusion.1
  12.9 0.1 reshape.99
  13.0 82.9 %all_to_all.55 = bf16[32,1,36,256]{3,2,1,0:T(8,128)(2,1)S(1)} all-to-all(bf16[32,1,36,256]{3,2,1,0:T(8,128)(2,1)S(1)} %bitcast.35), channel_id=1, replica_groups=mesh['grp'=2,'fs_0'=16,'fs_1'=2,'tp'=8] {'fs_0','fs_1'}, dimensions={0} | all-to-all | bytes 1179648 | tf_op jit(solution)/shard_map/all_to_all | solution.py:65
  95.9 0.9 squeeze.3
  96.9 0.1 all-gather.4.cloned.1.call-update
  96.9 0.0 copy-done.3
  96.9 0.0 copy-done.5
  96.9 2.3 multiply_convert_fusion
  99.2 37.1 %all_to_all.56 = bf16[32,64,128]{2,1,0:T(8,128)(2,1)S(1)} all-to-all(bf16[32,64,128]{2,1,0:T(8,128)(2,1)S(1)} %get-tuple-element.7), channel_id=1, replica_groups=mesh['grp'=2,'fs_0'=16,'fs_1'=2,'tp'=8] {'fs_0','fs_1'}, dimensions={0} | all-to-all | bytes 1048576 | tf_op jit(solution)/shard_map/all_to_all | solution.py:53
  136.3 4.8 %all-to-all-start.1 = ((bf16[32,64,128]{2,1,0:T(8,128)(2,1)}), bf16[32,64,128]{2,1,0:T(8,128)(2,1)S(1)}, u32[]{:S(2)}, u32[]{:S(2)}) async-start(bf16[32,64,128]{2,1,0:T(8,128)(2,1)} %get-tuple-element.6), calls=%async_computation.1 | async-start | bytes 1048576 | tf_op jit(solution)/shard_map/all_to_all | solution.py:54
  141.1 0.1 all-gather.6.cloned.1.call-start
  141.2 22.0 %all-gather.4.cloned.1.call-done = bf16[1,1152,2048]{2,1,0:T(8,128)(2,1)} async-done(((bf16[1,1152,256]{2,1,0:T(8,128)(2,1)}), bf16[1,1152,2048]{2,1,0:T(8,128)(2,1)}) %all-gather.4.cloned.1.call-update) | async-done | bytes 4718608 | tf_op jit(solution)/shard_map/all_gather | solution.py:66
  163.2 0.0 copy-start.1
  163.2 3.5 %fusion = f32[1152]{0:T(1024)S(1)} fusion(bf16[1,1152,2048]{2,1,0:T(8,128)(2,1)} %all-gather.4.cloned.1.call-done), kind=kLoop, calls=%fused_computation.3 | loop fusion | flops 7076736 | bytes 4723200 | tf_op jit(solution)/shard_map/reduce_sum | solution.py:40
  166.7 0.3 copy-done.1
  167.0 1.5 fusion.6
  168.5 5.8 %all-to-all-done.1 = bf16[32,64,128]{2,1,0:T(8,128)(2,1)S(1)} async-done(((bf16[32,64,128]{2,1,0:T(8,128)(2,1)}), bf16[32,64,128]{2,1,0:T(8,128)(2,1)S(1)}, u32[]{:S(2)}, u32[]{:S(2)}) %all-to-all-start.1) | async-done | bytes 524320 | tf_op jit(solution)/shard_map/all_to_all | solution.py:54
  174.3 0.0 copy-start.2
  174.3 4.6 %fusion.4 = bf16[1152,128]{1,0:T(8,128)(2,1)} fusion(bf16[2048,128]{1,0:T(8,128)(2,1)S(1)} %bitcast.38, bf16[1,1152,2048]{2,1,0:T(8,128)(2,1)} %all-gather.4.cloned.1.call-done, f32[1152]{0:T(1024)S(1)} %add_rsqrt_fusion, f32[1152,128]{1,0:T(8,128)S(1)} %fusion.6), kind=kOutput, calls=%fused_computation.11 | convolution fusion | flops 611942400 | bytes 6132224 | tf_op jit(solution)/shard_map/erd,edh->erh/dot_general | solution.py:70
  178.9 0.1 all-gather.6.cloned.1.call-update
  178.9 0.0 copy-done.2
  179.0 0.1 convert_element_type.42
  179.0 38.7 %all_to_all.57 = bf16[32,32,256]{2,1,0:T(8,128)(2,1)S(1)} all-to-all(bf16[32,32,256]{2,1,0:T(8,128)(2,1)S(1)} %convert_element_type.42), channel_id=1, replica_groups=mesh['grp'=2,'fs_0'=16,'fs_1'=2,'tp'=8] {'fs_0','fs_1'}, dimensions={0} | all-to-all | bytes 1048576 | tf_op jit(solution)/shard_map/all_to_all | solution.py:72
  217.8 9.2 %all-gather.6.cloned.1.call-done = bf16[1152,1024]{1,0:T(8,128)(2,1)} async-done(((bf16[1152,128]{1,0:T(8,128)(2,1)}), bf16[1152,1024]{1,0:T(8,128)(2,1)}) %all-gather.6.cloned.1.call-update) | async-done | bytes 2359312 | tf_op jit(solution)/shard_map/all_gather | solution.py:75
  226.9 2.4 convolution_convert_fusion
  229.4 0.0 copy-start.4
  229.4 0.1 reshape_transpose_reshape_reshape.3
  229.5 0.2 copy.46
  229.7 4.2 %all_to_all.58 = bf16[16,2,1,1,36,256]{5,0,4,3,2,1:T(8,128)(2,1)S(1)} all-to-all(bf16[16,2,1,1,36,256]{5,0,4,3,2,1:T(8,128)(2,1)S(1)} %copy.46), channel_id=1, replica_groups=mesh['grp'=2,'fs_0'=16,'fs_1'=2,'tp'=8] {'fs_1'}, dimensions={1} | all-to-all | bytes 1179648 | tf_op jit(solution)/shard_map/all_to_all | solution.py:28
  233.9 1.4 copy.47
  235.3 13.1 %all-to-all-start.5 = ((bf16[16,2,1,1,36,256]{5,1,4,3,2,0:T(2,128)(2,1)}), bf16[16,2,1,1,36,256]{5,1,4,3,2,0:T(2,128)(2,1)S(1)}, u32[]{:S(2)}, u32[]{:S(2)}) async-start(bf16[16,2,1,1,36,256]{5,1,4,3,2,0:T(2,128)(2,1)} %copy.47), calls=%async_computation.5 | async-start | bytes 1179648 | tf_op jit(solution)/shard_map/all_to_all | solution.py:28
  248.4 0.1 copy.49
  248.6 0.1 reshape.107
  248.7 0.0 copy-done.4
  248.7 0.1 copy.40
  248.9 30.4 %all-to-all-done.5 = bf16[16,2,1,1,36,256]{5,1,4,3,2,0:T(2,128)(2,1)S(1)} async-done(((bf16[16,2,1,1,36,256]{5,1,4,3,2,0:T(2,128)(2,1)}), bf16[16,2,1,1,36,256]{5,1,4,3,2,0:T(2,128)(2,1)S(1)}, u32[]{:S(2)}, u32[]{:S(2)}) %all-to-all-start.5) | async-done | bytes 589856 | tf_op jit(solution)/shard_map/all_to_all | solution.py:28
  279.3 0.1 copy.48
  279.3 0.1 reshape_reshape_reshape.3
  279.5 2.7 gather_fusion
  282.1 0.4 reshape.117
  282.5 1.7 multiply_reduce_fusion
  284.2 0.8 copy.55
  285.0 0.8 copy.56
  285.8 0.8 copy.57
  (4 shorter events, 0.0 us)
Async XLA Ops:
  7.2 5.2 %copy-start = (bf16[384,256]{1,0:T(8,128)(2,1)S(1)}, bf16[384,256]{1,0:T(8,128)(2,1)}, u32[]{:S(2)}) copy-start(bf16[384,256]{1,0:T(8,128)(2,1)} %param.7) | copy-start | bytes 589828
  7.2 89.7 %copy-start.3 = (f32[32,64,128]{2,1,0:T(8,128)S(1)}, f32[32,64,128]{2,1,0:T(8,128)}, u32[]{:S(2)}) copy-start(f32[32,64,128]{2,1,0:T(8,128)} %param.10) | copy-start | bytes 3145732
  7.2 89.7 %copy-start.5 = (f32[64]{0:T(128)S(1)}, f32[64]{0:T(128)}, u32[]{:S(2)}) copy-start(f32[64]{0:T(128)} %param.8) | copy-start | bytes 772
  7.2 156.0 %all-gather.4.cloned.1.call-start = ((), (), s32[]{:S(2)}) async-start(), calls=%async_computation.6 | async-start | bytes 5308416 | tf_op jit(solution)/shard_map/all_gather | solution.py:66
  136.3 38.0 %all-to-all-start.1 = ((bf16[32,64,128]{2,1,0:T(8,128)(2,1)}), bf16[32,64,128]{2,1,0:T(8,128)(2,1)S(1)}, u32[]{:S(2)}, u32[]{:S(2)}) async-start(bf16[32,64,128]{2,1,0:T(8,128)(2,1)} %get-tuple-element.6), calls=%async_computation.1 | async-start | bytes 1048576 | tf_op jit(solution)/shard_map/all_to_all | solution.py:54
  141.1 85.8 %all-gather.6.cloned.1.call-start = ((), (), s32[]{:S(2)}) async-start(), calls=%async_computation.7 | async-start | bytes 2654208 | tf_op jit(solution)/shard_map/all_gather | solution.py:75
  163.2 3.8 %copy-start.1 = (bf16[1,1152,2048]{2,1,0:T(8,128)(2,1)S(1)}, bf16[1,1152,2048]{2,1,0:T(8,128)(2,1)}, u32[]{:S(2)}) copy-start(bf16[1,1152,2048]{2,1,0:T(8,128)(2,1)} %all-gather.4.cloned.1.call-done) | copy-start | bytes 14155780
  174.3 4.7 %copy-start.2 = (f32[32,32,256]{2,1,0:T(8,128)S(1)}, f32[32,32,256]{2,1,0:T(8,128)}, u32[]{:S(2)}) copy-start(f32[32,32,256]{2,1,0:T(8,128)} %param.11) | copy-start | bytes 3145732
  229.4 19.4 %copy-start.4 = (f32[384,2]{0,1:T(2,128)S(1)}, f32[384,2]{0,1:T(2,128)}, u32[]{:S(2)}) copy-start(f32[384,2]{0,1:T(2,128)} %param.13) | copy-start | bytes 9220
  235.3 43.9 %all-to-all-start.5 = ((bf16[16,2,1,1,36,256]{5,1,4,3,2,0:T(2,128)(2,1)}), bf16[16,2,1,1,36,256]{5,1,4,3,2,0:T(2,128)(2,1)S(1)}, u32[]{:S(2)}, u32[]{:S(2)}) async-start(bf16[16,2,1,1,36,256]{5,1,4,3,2,0:T(2,128)(2,1)} %copy.47), calls=%async_computation.5 | async-start | bytes 1179648 | tf_op jit(solution)/shard_map/all_to_all | solution.py:28
Sparse Core Ops, SparseCore 0:
  97.0 66.1 all-gather.3
  179.1 47.8 all-gather.5
where the time goes:
time: 294 us; the launch traced here: 293 us
  blocking collectives  163 us (55%)
  waiting for transfers between devices  67.5 us (23%)
  starting transfers between devices  18 us (6%)
  between operations  14.3 us (5%)
  other arithmetic  10.9 us (4%)
  local copies, waits for them, and re-layouts  10.8 us (4%)
  matrix products  8.96 us (3%)
    all_to_all x1, blocking collectives, shards(): lax.all_to_all(outbound, FS, split_axis=0, concat_axis=2, tiled=True)[0]  82.9 us
    all_to_all x1, blocking collectives, shards(): lax.all_to_all(down_low, FS, split_axis=0, concat_axis=1, tiled=True)  38.7 us
    all_to_all x1, blocking collectives, shards(): lax.all_to_all(gate_low, FS, split_axis=0, concat_axis=1, tiled=True)  37.1 us
    all_to_all x1, waiting for transfers between devices, exchange_in_order(): lax.all_to_all(blocks, axes[k], split_axis=k, concat_axis=k, tiled=True)  30.4 us
    all_gather x1, waiting for transfers between devices, shards(): expert_rows = normalize(lax.all_gather(arrived, 'tp', axis=2, tiled=True))  22 us
    all_to_all x1, starting transfers between devices, exchange_in_order(): lax.all_to_all(blocks, axes[k], split_axis=k, concat_axis=k, tiled=True)  13.1 us
    all_gather x1, waiting for transfers between devices, shards(): lax.all_gather(hidden, 'tp', axis=2, tiled=True)  9.16 us
  transfers between devices with their start and end apart: 4, of which 4 were waited for; matrix products, arithmetic and copies ran while one was open for 3% of the time, Pallas kernels for 0%

commit v1 on v0

--- a/solution.py
+++ b/solution.py
@@ -63,7 +63,11 @@
     outbound = jnp.dot(select, tokens, preferred_element_type=jnp.float32).astype(jnp.bfloat16)
     outbound = outbound.reshape(n_shards, local_experts, CAP, outbound.shape[1])
     arrived = lax.all_to_all(outbound, FS, split_axis=0, concat_axis=2, tiled=True)[0]
-    expert_rows = normalize(lax.all_gather(arrived, "tp", axis=2, tiled=True))
+    expert_rows = normalize(
+        jnp.concatenate(
+            lax.all_to_all(jnp.stack([arrived] * lax.axis_size("tp")), "tp", 0, 0), axis=2
+        )
+    )
     gate_part = jnp.einsum(
         "erd,edh->erh", expert_rows, gate_serve, preferred_element_type=jnp.float32
     )

time: 294 us -> 404 us (1.37)
  waiting for transfers between devices: 67.5 us -> 130 us
  starting transfers between devices: 18 us -> 67.5 us
  blocking collectives: 163 us -> 155 us
  local copies, waits for them, and re-layouts: 10.8 us -> 15.4 us
    all_to_all x0 -> x2, waiting for transfers between devices: none -> 70.1 us  [the longest x1 37.4 us: shards(): lax.all_to_all(outbound, FS, split_axis=0, concat_axis=2, tiled=True)[0]]
    all_to_all x0 -> x2, starting transfers between devices: none -> 49.3 us  [the longest x1 44.4 us: shards(): lax.all_to_all(outbound, FS, split_axis=0, concat_axis=2, tiled=True)[0]]
    all_gather x1 -> x0, waiting for transfers between devices: 22 us -> none  [shards(): expert_rows = normalize(lax.all_gather(arrived, 'tp', axis=2, tiled=True))]
    all_to_all x1, waiting for transfers between devices: 5.82 us -> 23.6 us  [shards(): lax.all_to_all(up_low, FS, split_axis=0, concat_axis=1, tiled=True)]
    all_to_all x2 -> x1, blocking collectives: 120 us -> 113 us  [shards(): lax.all_to_all(jnp.stack([arrived] * lax.axis_size('tp')), 'tp', 0, 0)]
  transfers between devices with their start and end apart: 4 -> 5, of which waited for: 4 -> 5; matrix products, arithmetic and copies ran while one was open for 3% -> 2% of each run, Pallas kernels for 0% -> 0%
where the time goes in v1:
time: 404 us; the launch traced here: 403 us
  blocking collectives  155 us (38%)
  waiting for transfers between devices  130 us (32%)
  starting transfers between devices  67.5 us (17%)
  local copies, waits for them, and re-layouts  15.4 us (4%)
  between operations  14.4 us (4%)
  other arithmetic  10.6 us (3%)
  matrix products  10.3 us (3%)
    all_to_all x1, blocking collectives, shards(): lax.all_to_all(jnp.stack([arrived] * lax.axis_size('tp')), 'tp', 0, 0)  113 us
    all_to_all x1, starting transfers between devices, shards(): lax.all_to_all(outbound, FS, split_axis=0, concat_axis=2, tiled=True)[0]  44.4 us
    all_to_all x1, waiting for transfers between devices, shards(): lax.all_to_all(outbound, FS, split_axis=0, concat_axis=2, tiled=True)[0]  37.4 us
    all_to_all x1, blocking collectives, shards(): lax.all_to_all(down_low, FS, split_axis=0, concat_axis=1, tiled=True)  37.3 us
    all_to_all x1, waiting for transfers between devices, shards(): lax.all_to_all(gate_low, FS, split_axis=0, concat_axis=1, tiled=True)  32.8 us
    all_to_all x1, waiting for transfers between devices, exchange_in_order(): lax.all_to_all(blocks, axes[k], split_axis=k, concat_axis=k, tiled=True)  30.3 us
    all_to_all x1, waiting for transfers between devices, shards(): lax.all_to_all(up_low, FS, split_axis=0, concat_axis=1, tiled=True)  23.6 us
    all_to_all x1, starting transfers between devices, exchange_in_order(): lax.all_to_all(blocks, axes[k], split_axis=k, concat_axis=k, tiled=True)  13.4 us
  transfers between devices with their start and end apart: 5, of which 5 were waited for; matrix products, arithmetic and copies ran while one was open for 2% of the time, Pallas kernels for 0%

profile of v1, /device:TPU:66, one launch (start us, length us, event | category | flops | bytes accessed | tf_op | source)
XLA Modules:
  0.0 403.3 jit_solution(10945942297219220695)
XLA Ops:
  7.2 0.0 copy-start
  7.2 0.0 copy-start.4
  7.2 0.0 copy-start.7
  7.2 0.0 copy-start.5
  7.2 1.0 copy.49
  8.2 0.1 eq.43
  8.3 0.1 eq.39
  8.5 1.7 reduce-window.6
  10.3 0.3 slice_reduce_fusion
  10.5 0.1 fusion.7
  10.7 0.2 reduce_sum.30
  10.8 0.1 copy.52
  10.9 0.7 compare_select_fusion
  11.6 0.8 fusion.1
  12.4 0.0 copy-done
  12.4 0.5 convolution_convert_fusion.1
  12.9 1.0 reshape.167
  13.8 44.4 %all-to-all-start.3 = ((bf16[32,1,36,256]{3,2,1,0:T(8,128)(2,1)}), bf16[32,1,36,256]{3,2,1,0:T(8,128)(2,1)S(1)}, u32[]{:S(2)}, u32[]{:S(2)}) async-start(bf16[32,1,36,256]{3,2,1,0:T(8,128)(2,1)} %bitcast.4), calls=%async_computation.3 | async-start | bytes 1310720 | tf_op jit(solution)/shard_map/all_to_all | solution.py:65
  58.3 0.0 copy-done.4
  58.3 0.0 copy-done.7
  58.3 0.0 copy-done.5
  58.3 1.3 multiply_convert_fusion.1
  59.6 37.4 %all-to-all-done.3 = bf16[32,1,36,256]{3,2,1,0:T(8,128)(2,1)S(1)} async-done(((bf16[32,1,36,256]{3,2,1,0:T(8,128)(2,1)}), bf16[32,1,36,256]{3,2,1,0:T(8,128)(2,1)S(1)}, u32[]{:S(2)}, u32[]{:S(2)}) %all-to-all-start.3) | async-done | bytes 589856 | tf_op jit(solution)/shard_map/all_to_all | solution.py:65
  97.0 4.8 %all-to-all-start = ((bf16[32,64,128]{2,1,0:T(8,128)(2,1)}), bf16[32,64,128]{2,1,0:T(8,128)(2,1)S(1)}, u32[]{:S(2)}, u32[]{:S(2)}) async-start(bf16[32,64,128]{2,1,0:T(8,128)(2,1)} %get-tuple-element.7), calls=%async_computation | async-start | bytes 1048576 | tf_op jit(solution)/shard_map/all_to_all | solution.py:53
  101.8 0.1 all_to_all.52
  101.9 0.3 copy.54
  102.2 32.8 %all-to-all-done = bf16[32,64,128]{2,1,0:T(8,128)(2,1)S(1)} async-done(((bf16[32,64,128]{2,1,0:T(8,128)(2,1)}), bf16[32,64,128]{2,1,0:T(8,128)(2,1)S(1)}, u32[]{:S(2)}, u32[]{:S(2)}) %all-to-all-start) | async-done | bytes 524320 | tf_op jit(solution)/shard_map/all_to_all | solution.py:53
  135.0 0.6 stack.3
  135.6 113.4 %all_to_all.63 = bf16[8,1,1152,256]{2,3,1,0:T(8,128)(2,1)} all-to-all(bf16[8,1,1152,256]{2,3,1,0:T(8,128)(2,1)S(1)} %stack.3), channel_id=1, replica_groups=mesh['grp'=2,'fs_0'=16,'fs_1'=2,'tp'=8] {'tp'}, dimensions={0} | all-to-all | bytes 9437184 | tf_op jit(solution)/shard_map/all_to_all | solution.py:68
  249.0 4.8 %all-to-all-start.1 = ((bf16[32,64,128]{2,1,0:T(8,128)(2,1)}), bf16[32,64,128]{2,1,0:T(8,128)(2,1)S(1)}, u32[]{:S(2)}, u32[]{:S(2)}) async-start(bf16[32,64,128]{2,1,0:T(8,128)(2,1)} %get-tuple-element.6), calls=%async_computation.1 | async-start | bytes 1048576 | tf_op jit(solution)/shard_map/all_to_all | solution.py:54
  253.8 0.1 all-gather.3.cloned.1.call-start
  253.9 0.0 copy-start.2
  253.9 3.5 multiply_reduce_fusion
  257.4 0.3 copy-done.2
  257.6 0.6 bitcast_convert_fusion
  258.3 0.0 copy-start.1
  258.3 3.6 copy-done.1
  261.9 1.4 fusion.4
  263.3 23.6 %all-to-all-done.1 = bf16[32,64,128]{2,1,0:T(8,128)(2,1)S(1)} async-done(((bf16[32,64,128]{2,1,0:T(8,128)(2,1)}), bf16[32,64,128]{2,1,0:T(8,128)(2,1)S(1)}, u32[]{:S(2)}, u32[]{:S(2)}) %all-to-all-start.1) | async-done | bytes 524320 | tf_op jit(solution)/shard_map/all_to_all | solution.py:54
  287.0 5.9 %fusion.2 = bf16[1152,128]{1,0:T(8,128)(2,1)} fusion(bf16[2048,128]{1,0:T(8,128)(2,1)S(1)} %bitcast.46, f32[1,1152,1,1,1,1,2048]{1,6,5,4,3,2,0:T(8,128)} %bitcast.45, f32[1152]{0:T(1024)S(1)} %add_rsqrt_fusion, f32[1152,128]{1,0:T(8,128)S(1)} %fusion.4), kind=kOutput, calls=%fused_computation.10 | convolution fusion | flops 609583104 | bytes 10850816 | tf_op jit(solution)/shard_map/erd,edh->erh/dot_general | solution.py:74
  292.9 0.1 all-gather.3.cloned.1.call-update
  293.0 0.0 copy-done.3
  293.0 0.1 convert_element_type.97
  293.1 37.3 %all_to_all.64 = bf16[32,32,256]{2,1,0:T(8,128)(2,1)S(1)} all-to-all(bf16[32,32,256]{2,1,0:T(8,128)(2,1)S(1)} %convert_element_type.97), channel_id=1, replica_groups=mesh['grp'=2,'fs_0'=16,'fs_1'=2,'tp'=8] {'fs_0','fs_1'}, dimensions={0} | all-to-all | bytes 1048576 | tf_op jit(solution)/shard_map/all_to_all | solution.py:76
  330.3 6.2 %all-gather.3.cloned.1.call-done = bf16[1152,1024]{1,0:T(8,128)(2,1)} async-done(((bf16[1152,128]{1,0:T(8,128)(2,1)}), bf16[1152,1024]{1,0:T(8,128)(2,1)}) %all-gather.3.cloned.1.call-update) | async-done | bytes 2359312 | tf_op jit(solution)/shard_map/all_gather | solution.py:79
  336.5 2.4 convolution_convert_fusion
  338.9 0.0 copy-start.6
  338.9 0.1 reshape_transpose_reshape_reshape.3
  339.0 0.2 copy.57
  339.2 4.2 %all_to_all.65 = bf16[16,2,1,1,36,256]{5,0,4,3,2,1:T(8,128)(2,1)S(1)} all-to-all(bf16[16,2,1,1,36,256]{5,0,4,3,2,1:T(8,128)(2,1)S(1)} %copy.57), channel_id=1, replica_groups=mesh['grp'=2,'fs_0'=16,'fs_1'=2,'tp'=8] {'fs_1'}, dimensions={1} | all-to-all | bytes 1179648 | tf_op jit(solution)/shard_map/all_to_all | solution.py:28
  343.5 1.4 copy.58
  344.9 13.4 %all-to-all-start.6 = ((bf16[16,2,1,1,36,256]{5,1,4,3,2,0:T(2,128)(2,1)}), bf16[16,2,1,1,36,256]{5,1,4,3,2,0:T(2,128)(2,1)S(1)}, u32[]{:S(2)}, u32[]{:S(2)}) async-start(bf16[16,2,1,1,36,256]{5,1,4,3,2,0:T(2,128)(2,1)} %copy.58), calls=%async_computation.6 | async-start | bytes 1179648 | tf_op jit(solution)/shard_map/all_to_all | solution.py:28
  358.3 0.1 copy.60
  358.4 0.1 reshape.175
  358.6 0.1 copy.48
  358.7 30.3 %all-to-all-done.6 = bf16[16,2,1,1,36,256]{5,1,4,3,2,0:T(2,128)(2,1)S(1)} async-done(((bf16[16,2,1,1,36,256]{5,1,4,3,2,0:T(2,128)(2,1)}), bf16[16,2,1,1,36,256]{5,1,4,3,2,0:T(2,128)(2,1)S(1)}, u32[]{:S(2)}, u32[]{:S(2)}) %all-to-all-start.6) | async-done | bytes 589856 | tf_op jit(solution)/shard_map/all_to_all | solution.py:28
  389.1 0.1 copy.59
  389.1 0.1 reshape_reshape_reshape.3
  389.3 2.7 gather_fusion
  391.9 0.4 reshape.185
  392.3 1.7 multiply_reduce_fusion.1
  394.0 0.8 copy.66
  394.8 0.8 copy.67
  395.6 0.8 copy.68
  (6 shorter events, 0.1 us)
Async XLA Ops:
  7.2 5.2 %copy-start = (bf16[384,256]{1,0:T(8,128)(2,1)S(1)}, bf16[384,256]{1,0:T(8,128)(2,1)}, u32[]{:S(2)}) copy-start(bf16[384,256]{1,0:T(8,128)(2,1)} %param.7) | copy-start | bytes 589828
  7.2 51.1 %copy-start.4 = (f32[32,64,128]{2,1,0:T(8,128)S(1)}, f32[32,64,128]{2,1,0:T(8,128)}, u32[]{:S(2)}) copy-start(f32[32,64,128]{2,1,0:T(8,128)} %param.10) | copy-start | bytes 3145732
  7.2 51.1 %copy-start.7 = (f32[64]{0:T(128)S(1)}, f32[64]{0:T(128)}, u32[]{:S(2)}) copy-start(f32[64]{0:T(128)} %param.8) | copy-start | bytes 772
  7.2 51.1 %copy-start.5 = (f32[32,64,128]{2,1,0:T(8,128)S(1)}, f32[32,64,128]{2,1,0:T(8,128)}, u32[]{:S(2)}) copy-start(f32[32,64,128]{2,1,0:T(8,128)} %param.9) | copy-start | bytes 3145732
  13.8 83.1 %all-to-all-start.3 = ((bf16[32,1,36,256]{3,2,1,0:T(8,128)(2,1)}), bf16[32,1,36,256]{3,2,1,0:T(8,128)(2,1)S(1)}, u32[]{:S(2)}, u32[]{:S(2)}) async-start(bf16[32,1,36,256]{3,2,1,0:T(8,128)(2,1)} %bitcast.4), calls=%async_computation.3 | async-start | bytes 1310720 | tf_op jit(solution)/shard_map/all_to_all | solution.py:65
  97.0 38.0 %all-to-all-start = ((bf16[32,64,128]{2,1,0:T(8,128)(2,1)}), bf16[32,64,128]{2,1,0:T(8,128)(2,1)S(1)}, u32[]{:S(2)}, u32[]{:S(2)}) async-start(bf16[32,64,128]{2,1,0:T(8,128)(2,1)} %get-tuple-element.7), calls=%async_computation | async-start | bytes 1048576 | tf_op jit(solution)/shard_map/all_to_all | solution.py:53
  249.0 38.0 %all-to-all-start.1 = ((bf16[32,64,128]{2,1,0:T(8,128)(2,1)}), bf16[32,64,128]{2,1,0:T(8,128)(2,1)S(1)}, u32[]{:S(2)}, u32[]{:S(2)}) async-start(bf16[32,64,128]{2,1,0:T(8,128)(2,1)} %get-tuple-element.6), calls=%async_computation.1 | async-start | bytes 1048576 | tf_op jit(solution)/shard_map/all_to_all | solution.py:54
  253.8 82.7 %all-gather.3.cloned.1.call-start = ((), (), s32[]{:S(2)}) async-start(), calls=%async_computation.7 | async-start | bytes 2654208 | tf_op jit(solution)/shard_map/all_gather | solution.py:79
  253.9 3.8 copy-start.2
  258.3 3.6 copy-start.1
  287.0 6.0 %copy-start.3 = (f32[32,32,256]{2,1,0:T(8,128)S(1)}, f32[32,32,256]{2,1,0:T(8,128)}, u32[]{:S(2)}) copy-start(f32[32,32,256]{2,1,0:T(8,128)} %param.11) | copy-start | bytes 3145732
  338.9 19.6 %copy-start.6 = (f32[384,2]{0,1:T(2,128)S(1)}, f32[384,2]{0,1:T(2,128)}, u32[]{:S(2)}) copy-start(f32[384,2]{0,1:T(2,128)} %param.13) | copy-start | bytes 9220
  344.9 44.2 %all-to-all-start.6 = ((bf16[16,2,1,1,36,256]{5,1,4,3,2,0:T(2,128)(2,1)}), bf16[16,2,1,1,36,256]{5,1,4,3,2,0:T(2,128)(2,1)S(1)}, u32[]{:S(2)}, u32[]{:S(2)}) async-start(bf16[16,2,1,1,36,256]{5,1,4,3,2,0:T(2,128)(2,1)} %copy.58), calls=%async_computation.6 | async-start | bytes 1179648 | tf_op jit(solution)/shard_map/all_to_all | solution.py:28
Sparse Core Ops, SparseCore 0:
  293.1 43.3 all-gather.2
